TPU v7x, 32 devices: a whole 2x2x4 slice. The times are simulated.
32 devices in a mesh: gr: 2 (over x), fs: 4 (over z), tp: 4 (over y, core).
Axes of the slice: x: 2, y: 2, z: 4, core: 2. Of those that a mesh axis runs over, the one named last changes fastest.
Arguments:
- tokens: bfloat16 [4096, 2048], P(('gr', 'fs', 'tp')), may hold values from -6 to 6
- norm_gain: float32 [2048], P('fs'), may hold values from 0.1 to 1.9
- gate_master: float32 [16, 2048, 256], P(None, 'fs', ('gr', 'tp')), may hold values from -0.125 to 0.125
- up_master: float32 [16, 2048, 256], P(None, 'fs', ('gr', 'tp')), may hold values from -0.125 to 0.125
- down_master: float32 [16, 256, 2048], P(None, 'fs', ('gr', 'tp')), may hold values from -0.375 to 0.375
- route_group: int32 [4096], P(('gr', 'fs', 'tp')), may hold values from 0 to 3
- route_expert: int32 [4096, 2], P(('gr', 'fs', 'tp')), may hold values from 0 to 3, all different within a row
- route_weight: float32 [4096, 2], P(('gr', 'fs', 'tp')), may hold values from 0.1 to 1
Outputs:
- gate_new: bfloat16 [16, 2048, 256], P(('fs', 'tp'))
- up_new: bfloat16 [16, 2048, 256], P(('fs', 'tp'))
- down_new: bfloat16 [16, 256, 2048], P(('fs', 'tp'))
- mixed: bfloat16 [4096, 2048], P(('gr', 'fs', 'tp'))
Inputs may be any that keep to these rules, and one draw needn't show every extreme that they name: `route_expert`: the 2 entries of a row are different.
All inputs are finite; a program needn't handle non-finite values.
Results may differ from a plain program's by a relative error of at most 0.0086.
Values may be sent and summed in bfloat16 or wider, within the bound.
A program may use at most 64 MiB of HBM per device.

v0:
```python
import jax
import jax.numpy as jnp
from jax import lax
from jax.sharding import PartitionSpec as P

E_GROUPS = 4
TOP = 2


def body(
    tokens, norm_gain, gate_master, up_master, down_master, route_group, route_expert, route_weight
):
    n_fs = lax.axis_size("fs")
    n_tp = lax.axis_size("tp")
    n_gr = lax.axis_size("gr")
    experts = n_fs * n_tp
    per_group = experts // E_GROUPS
    gate_cast = (gate_master * norm_gain[None, :, None]).astype(jnp.bfloat16)
    up_cast = (up_master * norm_gain[None, :, None]).astype(jnp.bfloat16)
    down_cast = down_master.astype(jnp.bfloat16)

    def to_grid(tile):
        return tile.reshape((n_fs, n_tp, 1, tile.shape[1], tile.shape[2]))

    grids = (
        to_grid(jnp.swapaxes(gate_cast, 1, 2)),
        to_grid(jnp.swapaxes(up_cast, 1, 2)),
        to_grid(down_cast),
    )
    grids = (
        lax.all_to_all(
            lax.all_to_all(grids[0], "fs", split_axis=0, concat_axis=4, tiled=True),
            "tp",
            split_axis=1,
            concat_axis=3,
            tiled=True,
        ),
        lax.all_to_all(
            lax.all_to_all(grids[1], "fs", split_axis=0, concat_axis=4, tiled=True),
            "tp",
            split_axis=1,
            concat_axis=3,
            tiled=True,
        ),
        lax.all_to_all(
            lax.all_to_all(grids[2], "fs", split_axis=0, concat_axis=4, tiled=True),
            "tp",
            split_axis=1,
            concat_axis=3,
            tiled=True,
        ),
    )
    grids = (
        lax.all_gather(grids[0], "gr", axis=2, tiled=True),
        lax.all_gather(grids[1], "gr", axis=2, tiled=True),
        lax.all_gather(grids[2], "gr", axis=2, tiled=True),
    )

    def rows_to_matrix(grid):
        hidden_units = grid.shape[2] * grid.shape[3]
        return jnp.swapaxes(grid.reshape(hidden_units, grid.shape[4]), 0, 1)[None]

    gate_new = rows_to_matrix(grids[0])
    up_new = rows_to_matrix(grids[1])
    grid = grids[2]
    f_local = grid.shape[3] // n_tp
    d_local = grid.shape[4] // n_fs
    parts = grid.reshape(n_gr, n_tp, f_local, n_fs, d_local)
    parts = jnp.transpose(parts, (3, 2, 0, 1, 4))
    down_new = parts.reshape(1, n_fs * f_local, n_gr * n_tp * d_local)
    width = tokens.shape[1]
    count = tokens.shape[0]
    floats = tokens.astype(jnp.float32)
    normed = (floats * lax.rsqrt(jnp.mean(floats * floats, axis=-1, keepdims=True) + 1e-06)).astype(
        jnp.bfloat16
    )
    capacity = 3 * count * TOP // (2 * experts)
    flat_ids = (route_group[:, None] * per_group + route_expert).reshape(-1)
    columns = lax.broadcasted_iota(jnp.int32, (flat_ids.shape[0], experts), 1)
    onehot = (flat_ids[:, None] == columns).astype(jnp.int32)
    rank = jnp.sum((jnp.cumsum(onehot, axis=0) - 1) * onehot, axis=1)
    dump = experts * capacity
    slot = jnp.where(rank < capacity, flat_ids * capacity + rank, dump)
    rows = jnp.repeat(normed, TOP, axis=0)
    outgoing = (
        jnp.zeros((dump + 1, width), jnp.bfloat16)
        .at[slot]
        .set(rows)[:-1]
        .reshape(experts, capacity, width)
    )
    block = lax.all_to_all(outgoing, ("fs", "tp"), split_axis=0, concat_axis=0, tiled=True)
    flat_rows = block.reshape(-1, width)
    gate = jnp.dot(flat_rows, gate_new[0], preferred_element_type=jnp.float32)
    upper = jnp.dot(flat_rows, up_new[0], preferred_element_type=jnp.float32)
    hidden = (jax.nn.silu(gate) * upper).astype(jnp.bfloat16)
    result = jnp.dot(hidden, down_new[0], preferred_element_type=jnp.float32).astype(jnp.bfloat16)
    outcome = result.reshape(block.shape)
    returned = lax.all_to_all(outcome, ("fs", "tp"), split_axis=0, concat_axis=0, tiled=True)
    table = jnp.concatenate(
        [returned.reshape(-1, width), jnp.zeros((1, width), jnp.bfloat16)], axis=0
    )
    picked = table[slot].reshape(count, TOP, width).astype(jnp.float32)
    mixed = jnp.sum(picked * route_weight[:, :, None], axis=1).astype(jnp.bfloat16)
    return (gate_new, up_new, down_new, mixed)


def solution(mesh):
    placed = (
        P(("gr", "fs", "tp"), None),
        P("fs"),
        P(None, "fs", ("gr", "tp")),
        P(None, "fs", ("gr", "tp")),
        P(None, "fs", ("gr", "tp")),
        P(("gr", "fs", "tp")),
        P(("gr", "fs", "tp"), None),
        P(("gr", "fs", "tp"), None),
    )
    return jax.shard_map(
        body,
        mesh=mesh,
        in_specs=placed,
        out_specs=(
            P(("fs", "tp"), None, None),
            P(("fs", "tp"), None, None),
            P(("fs", "tp"), None, None),
            P(("gr", "fs", "tp"), None),
        ),
        check_vma=False,
    )
```

profile of v0, /device:TPU:13, one launch (start us, length us, event | category | flops | bytes accessed | tf_op | source)
XLA Modules:
  0.0 240.0 jit_solution(1093380789958716760)
XLA Ops:
  7.2 2.6 %multiply_convert_fusion = (bf16[16,512,32]{1,2,0:T(8,128)(2,1)}, bf16[16,512,32]{1,2,0:T(8,128)(2,1)S(1)}) fusion(f32[16,512,32]{1,2,0:T(8,128)} %param.11, f32[512]{0:T(512)} %param.9, f32[16,512,32]{1,2,0:T(8,128)} %param.10), kind=kLoop, calls=%fused_computation.10 | loop fusion | flops 1048576 | bytes 3147776 | tf_op jit(solution)/shard_map/convert_element_type | solution.py:19
  9.8 16.6 %all_to_all.100 = bf16[4,4,1,32,512]{4,3,1,2,0:T(8,128)(2,1)S(1)} all-to-all(bf16[4,4,1,32,512]{4,3,1,2,0:T(8,128)(2,1)S(1)} %bitcast.88), channel_id=1, replica_groups=mesh['gr'=2,'fs'=4,'tp'=4] {'fs'}, dimensions={0} | all-to-all | bytes 1048576 | tf_op jit(solution)/shard_map/all_to_all | solution.py:32
  26.4 5.3 %all-to-all-start.2 = ((bf16[4,4,1,32,512]{4,3,1,2,0:T(8,128)(2,1)}), bf16[4,4,1,32,512]{4,3,1,2,0:T(8,128)(2,1)S(1)}, u32[]{:S(2)}, u32[]{:S(2)}) async-start(bf16[4,4,1,32,512]{4,3,1,2,0:T(8,128)(2,1)} %bitcast.11), calls=%async_computation.2 | async-start | bytes 1048576 | tf_op jit(solution)/shard_map/all_to_all | solution.py:39
  32.6 9.8 %all-to-all-done.2 = bf16[4,4,1,32,512]{4,3,1,2,0:T(8,128)(2,1)S(1)} async-done(((bf16[4,4,1,32,512]{4,3,1,2,0:T(8,128)(2,1)}), bf16[4,4,1,32,512]{4,3,1,2,0:T(8,128)(2,1)S(1)}, u32[]{:S(2)}, u32[]{:S(2)}) %all-to-all-start.2) | async-done | bytes 524320 | tf_op jit(solution)/shard_map/all_to_all | solution.py:39
  42.4 7.0 %all-to-all-start.4 = ((bf16[4,4,1,64,256]{4,3,1,2,0:T(8,128)(2,1)}), bf16[4,4,1,64,256]{4,3,1,2,0:T(8,128)(2,1)S(1)}, u32[]{:S(2)}, u32[]{:S(2)}) async-start(bf16[4,4,1,64,256]{4,3,1,2,0:T(8,128)(2,1)} %bitcast.20), calls=%async_computation.4 | async-start | bytes 1048576 | tf_op jit(solution)/shard_map/all_to_all | solution.py:46
  50.5 9.5 %all-to-all-done.4 = bf16[4,4,1,64,256]{4,3,1,2,0:T(8,128)(2,1)S(1)} async-done(((bf16[4,4,1,64,256]{4,3,1,2,0:T(8,128)(2,1)}), bf16[4,4,1,64,256]{4,3,1,2,0:T(8,128)(2,1)S(1)}, u32[]{:S(2)}, u32[]{:S(2)}) %all-to-all-start.4) | async-done | bytes 524320 | tf_op jit(solution)/shard_map/all_to_all | solution.py:46
  60.0 5.4 %all-to-all-start.1 = ((bf16[1,4,1,32,2048]{4,3,2,0,1:T(8,128)(2,1)}), bf16[1,4,1,32,2048]{4,3,2,0,1:T(8,128)(2,1)S(1)}, u32[]{:S(2)}, u32[]{:S(2)}) async-start(bf16[1,4,1,32,2048]{4,3,2,0,1:T(8,128)(2,1)} %bitcast.4), calls=%async_computation.1 | async-start | bytes 1048576 | tf_op jit(solution)/shard_map/all_to_all | solution.py:31
  67.0 5.3 %all-to-all-done.1 = bf16[1,4,1,32,2048]{4,3,2,0,1:T(8,128)(2,1)S(1)} async-done(((bf16[1,4,1,32,2048]{4,3,2,0,1:T(8,128)(2,1)}), bf16[1,4,1,32,2048]{4,3,2,0,1:T(8,128)(2,1)S(1)}, u32[]{:S(2)}, u32[]{:S(2)}) %all-to-all-start.1) | async-done | bytes 524320 | tf_op jit(solution)/shard_map/all_to_all | solution.py:31
  72.4 5.3 %all-to-all-start.3 = ((bf16[1,4,1,32,2048]{4,3,2,0,1:T(8,128)(2,1)}), bf16[1,4,1,32,2048]{4,3,2,0,1:T(8,128)(2,1)S(1)}, u32[]{:S(2)}, u32[]{:S(2)}) async-start(bf16[1,4,1,32,2048]{4,3,2,0,1:T(8,128)(2,1)} %bitcast.87), calls=%async_computation.3 | async-start | bytes 1048576 | tf_op jit(solution)/shard_map/all_to_all | solution.py:38
  78.7 6.0 %all-to-all-done.3 = bf16[1,4,1,32,2048]{4,3,2,0,1:T(8,128)(2,1)S(1)} async-done(((bf16[1,4,1,32,2048]{4,3,2,0,1:T(8,128)(2,1)}), bf16[1,4,1,32,2048]{4,3,2,0,1:T(8,128)(2,1)S(1)}, u32[]{:S(2)}, u32[]{:S(2)}) %all-to-all-start.3) | async-done | bytes 524320 | tf_op jit(solution)/shard_map/all_to_all | solution.py:38
  84.6 5.9 %all-to-all-start.5 = ((bf16[1,4,1,64,1024]{4,3,2,0,1:T(8,128)(2,1)}), bf16[1,4,1,64,1024]{4,3,2,0,1:T(8,128)(2,1)}, u32[]{:S(2)}, u32[]{:S(2)}) async-start(bf16[1,4,1,64,1024]{4,3,2,0,1:T(8,128)(2,1)} %bitcast.23), calls=%async_computation.5 | async-start | bytes 1048576 | tf_op jit(solution)/shard_map/all_to_all | solution.py:45
  92.4 2.6 %scatter_custom_fusion = bf16[385,2048]{1,0:T(8,128)(2,1)S(1)} fusion(s32[256]{0:T(256)S(1)} %bitcast.94, bf16[256,2048]{1,0:T(8,128)(2,1)S(1)} %reshape.146, bf16[]{:T(256)} %constant.11.clone.1), kind=kCustom, calls=%fused_computation.12 | custom fusion | bytes 1576962 | tf_op jit(solution)/shard_map/scatter | solution.py:88
  97.6 8.1 %all-to-all-start.6 = ((bf16[16,24,2048]{2,1,0:T(8,128)(2,1)}), bf16[16,24,2048]{2,1,0:T(8,128)(2,1)S(1)}, u32[]{:S(2)}, u32[]{:S(2)}) async-start(bf16[16,24,2048]{2,1,0:T(8,128)(2,1)} %bitcast.30), calls=%async_computation.6 | async-start | bytes 3145728 | tf_op jit(solution)/shard_map/all_to_all | solution.py:91
  108.0 21.9 %all-gather.8.cloned.1.call-done = bf16[1,1,2,256,1024]{4,3,1,0,2:T(8,128)(2,1)} async-done(((bf16[1,1,1,256,1024]{4,3,1,0,2:T(8,128)(2,1)}), bf16[1,1,2,256,1024]{4,3,1,0,2:T(8,128)(2,1)}) %all-gather.8.cloned.1.call-update) | async-done | bytes 1048592 | tf_op jit(solution)/shard_map/all_gather | solution.py:56
  129.9 2.6 %reshape.125 = bf16[2,4,64,4,256]{4,3,2,1,0:T(4,128)(2,1)} reshape(bf16[1,1,2,256,1024]{4,3,1,0,2:T(8,128)(2,1)} %all-gather.8.cloned.1.call-done) | data formatting | bytes 2097152 | tf_op jit(solution)/shard_map/reshape | solution.py:68
  132.5 2.0 copy.46
  136.1 17.2 %all-gather.4.cloned.1.call-done = bf16[1,1,2,128,2048]{4,3,1,0,2:T(8,128)(2,1)} async-done(((bf16[1,1,1,128,2048]{4,3,1,0,2:T(8,128)(2,1)}), bf16[1,1,2,128,2048]{4,3,1,0,2:T(8,128)(2,1)}) %all-gather.4.cloned.1.call-update) | async-done | bytes 1048592 | tf_op jit(solution)/shard_map/all_gather | solution.py:54
  155.2 21.6 %all-gather.6.cloned.1.call-done = bf16[1,1,2,128,2048]{4,3,1,0,2:T(8,128)(2,1)} async-done(((bf16[1,1,1,128,2048]{4,3,1,0,2:T(8,128)(2,1)}), bf16[1,1,2,128,2048]{4,3,1,0,2:T(8,128)(2,1)}) %all-gather.6.cloned.1.call-update) | async-done | bytes 1048592 | tf_op jit(solution)/shard_map/all_gather | solution.py:55
  176.8 4.5 %convolution_convert_fusion = bf16[384,2048]{1,0:T(8,128)(2,1)} fusion(bf16[256,2048]{1,0:T(8,128)(2,1)} %squeeze_reshape.3, bf16[384,2048]{1,0:T(8,128)(2,1)S(1)} %bitcast.77, bf16[256,2048]{1,0:T(8,128)(2,1)} %bitcast.90, f32[384,256]{1,0:T(8,128)S(1)} %fusion.15), kind=kOutput, calls=%fused_computation.2 | convolution fusion | flops 806682624 | bytes 5636096 | tf_op jit(solution)/shard_map/dot_general | solution.py:96
  181.3 6.6 %all-to-all-start.7 = ((bf16[16,24,2048]{2,1,0:T(8,128)(2,1)}), bf16[16,24,2048]{2,1,0:T(8,128)(2,1)S(1)}, u32[]{:S(2)}, u32[]{:S(2)}) async-start(bf16[16,24,2048]{2,1,0:T(8,128)(2,1)} %bitcast.89), calls=%async_computation.7 | async-start | bytes 3145728 | tf_op jit(solution)/shard_map/all_to_all | solution.py:98
  188.1 2.3 copy.42
  190.3 2.3 copy.38
  194.2 30.0 %all-to-all-done.7 = bf16[16,24,2048]{2,1,0:T(8,128)(2,1)S(1)} async-done(((bf16[16,24,2048]{2,1,0:T(8,128)(2,1)}), bf16[16,24,2048]{2,1,0:T(8,128)(2,1)S(1)}, u32[]{:S(2)}, u32[]{:S(2)}) %all-to-all-start.7) | async-done | bytes 1572896 | tf_op jit(solution)/shard_map/all_to_all | solution.py:98
  229.5 3.9 %multiply_reduce_fusion = bf16[128,2048]{1,0:T(8,128)(2,1)} fusion(f32[128,2,2048]{2,1,0:T(2,128)S(1)} %reshape.133, f32[128,2]{1,0:T(8,128)S(1)} %copy.52), kind=kLoop, calls=%fused_computation.3 | loop fusion | flops 786432 | bytes 2622464 | tf_op jit(solution)/shard_map/reduce_sum | solution.py:103
  (56 shorter events, 21.7 us)
Async XLA Ops:
  9.8 22.0 %copy-start.4 = (f32[16,64,256]{2,1,0:T(8,128)S(1)}, f32[16,64,256]{2,1,0:T(8,128)}, u32[]{:S(2)}) copy-start(f32[16,64,256]{2,1,0:T(8,128)} %param.12) | copy-start | bytes 3145732
  26.4 22.9 %copy-start.7 = (s32[128]{0:T(128)S(1)}, s32[128]{0:T(128)}, u32[]{:S(2)}) copy-start(s32[128]{0:T(128)} %param.13) | copy-start | bytes 1540
  26.4 22.9 %copy-start.6 = (s32[128,2]{0,1:T(2,128)S(1)}, s32[128,2]{0,1:T(2,128)}, u32[]{:S(2)}) copy-start(s32[128,2]{0,1:T(2,128)} %param.14) | copy-start | bytes 3076
  26.4 15.9 %all-to-all-start.2 = ((bf16[4,4,1,32,512]{4,3,1,2,0:T(8,128)(2,1)}), bf16[4,4,1,32,512]{4,3,1,2,0:T(8,128)(2,1)S(1)}, u32[]{:S(2)}, u32[]{:S(2)}) async-start(bf16[4,4,1,32,512]{4,3,1,2,0:T(8,128)(2,1)} %bitcast.11), calls=%async_computation.2 | async-start | bytes 1048576 | tf_op jit(solution)/shard_map/all_to_all | solution.py:39
  42.4 23.6 %copy-start.1 = (bf16[128,2048]{1,0:T(8,128)(2,1)S(1)}, bf16[128,2048]{1,0:T(8,128)(2,1)}, u32[]{:S(2)}) copy-start(bf16[128,2048]{1,0:T(8,128)(2,1)} %param.8) | copy-start | bytes 1572868
  42.4 17.6 %all-to-all-start.4 = ((bf16[4,4,1,64,256]{4,3,1,2,0:T(8,128)(2,1)}), bf16[4,4,1,64,256]{4,3,1,2,0:T(8,128)(2,1)S(1)}, u32[]{:S(2)}, u32[]{:S(2)}) async-start(bf16[4,4,1,64,256]{4,3,1,2,0:T(8,128)(2,1)} %bitcast.20), calls=%async_computation.4 | async-start | bytes 1048576 | tf_op jit(solution)/shard_map/all_to_all | solution.py:46
  60.0 12.3 %all-to-all-start.1 = ((bf16[1,4,1,32,2048]{4,3,2,0,1:T(8,128)(2,1)}), bf16[1,4,1,32,2048]{4,3,2,0,1:T(8,128)(2,1)S(1)}, u32[]{:S(2)}, u32[]{:S(2)}) async-start(bf16[1,4,1,32,2048]{4,3,2,0,1:T(8,128)(2,1)} %bitcast.4), calls=%async_computation.1 | async-start | bytes 1048576 | tf_op jit(solution)/shard_map/all_to_all | solution.py:31
  72.4 12.3 %copy-start.2 = (bf16[1,4,1,32,2048]{4,3,2,0,1:T(8,128)(2,1)}, bf16[1,4,1,32,2048]{4,3,2,0,1:T(8,128)(2,1)S(1)}, u32[]{:S(2)}) copy-start(bf16[1,4,1,32,2048]{4,3,2,0,1:T(8,128)(2,1)S(1)} %all-to-all-done.1) | copy-start | bytes 1572868
  72.4 12.3 %all-to-all-start.3 = ((bf16[1,4,1,32,2048]{4,3,2,0,1:T(8,128)(2,1)}), bf16[1,4,1,32,2048]{4,3,2,0,1:T(8,128)(2,1)S(1)}, u32[]{:S(2)}, u32[]{:S(2)}) async-start(bf16[1,4,1,32,2048]{4,3,2,0,1:T(8,128)(2,1)} %bitcast.87), calls=%async_computation.3 | async-start | bytes 1048576 | tf_op jit(solution)/shard_map/all_to_all | solution.py:38
  84.6 7.7 %copy-start.3 = (bf16[1,4,1,32,2048]{4,3,2,0,1:T(8,128)(2,1)}, bf16[1,4,1,32,2048]{4,3,2,0,1:T(8,128)(2,1)S(1)}, u32[]{:S(2)}) copy-start(bf16[1,4,1,32,2048]{4,3,2,0,1:T(8,128)(2,1)S(1)} %all-to-all-done.3) | copy-start | bytes 1572868
  84.6 13.0 %all-to-all-start.5 = ((bf16[1,4,1,64,1024]{4,3,2,0,1:T(8,128)(2,1)}), bf16[1,4,1,64,1024]{4,3,2,0,1:T(8,128)(2,1)}, u32[]{:S(2)}, u32[]{:S(2)}) async-start(bf16[1,4,1,64,1024]{4,3,2,0,1:T(8,128)(2,1)} %bitcast.23), calls=%async_computation.5 | async-start | bytes 1048576 | tf_op jit(solution)/shard_map/all_to_all | solution.py:45
  97.6 55.7 %all-to-all-start.6 = ((bf16[16,24,2048]{2,1,0:T(8,128)(2,1)}), bf16[16,24,2048]{2,1,0:T(8,128)(2,1)S(1)}, u32[]{:S(2)}, u32[]{:S(2)}) async-start(bf16[16,24,2048]{2,1,0:T(8,128)(2,1)} %bitcast.30), calls=%async_computation.6 | async-start | bytes 3145728 | tf_op jit(solution)/shard_map/all_to_all | solution.py:91
  105.7 24.1 %all-gather.8.cloned.1.call-start = ((), (), s32[]{:S(2)}) async-start(), calls=%async_computation.10 | async-start | bytes 1572864 | tf_op jit(solution)/shard_map/all_gather | solution.py:56
  106.5 46.8 %all-gather.4.cloned.1.call-start = ((), (), s32[]{:S(2)}) async-start(), calls=%async_computation.8 | async-start | bytes 1572864 | tf_op jit(solution)/shard_map/all_gather | solution.py:54
  107.2 69.5 %all-gather.6.cloned.1.call-start = ((), (), s32[]{:S(2)}) async-start(), calls=%async_computation.9 | async-start | bytes 1572864 | tf_op jit(solution)/shard_map/all_gather | solution.py:55
  181.3 6.6 %copy-start.5 = (f32[128,2]{0,1:T(2,128)S(1)}, f32[128,2]{0,1:T(2,128)}, u32[]{:S(2)}) copy-start(f32[128,2]{0,1:T(2,128)} %param.15) | copy-start | bytes 3076
  181.3 42.8 %all-to-all-start.7 = ((bf16[16,24,2048]{2,1,0:T(8,128)(2,1)}), bf16[16,24,2048]{2,1,0:T(8,128)(2,1)S(1)}, u32[]{:S(2)}, u32[]{:S(2)}) async-start(bf16[16,24,2048]{2,1,0:T(8,128)(2,1)} %bitcast.89), calls=%async_computation.7 | async-start | bytes 3145728 | tf_op jit(solution)/shard_map/all_to_all | solution.py:98
  224.1 1.2 copy-start
Sparse Core Ops, SparseCore 0:
  108.1 21.7 all-gather.7
  132.0 21.2 all-gather.3
  155.4 21.2 all-gather.5
where the time goes:
time: 241 us; the launch traced here: 240 us
  waiting for transfers between devices  125 us (52%)
  starting transfers between devices  43.7 us (18%)
  local copies, waits for them, and re-layouts  26.2 us (11%)
  blocking collectives  16.6 us (7%)
  between operations  13.9 us (6%)
  other arithmetic  8.49 us (4%)
  matrix products  6.36 us (3%)
    all_to_all x1, waiting for transfers between devices, body(): lax.all_to_all(outcome, ('fs', 'tp'), split_axis=0, concat_axis=0, tiled=...  30 us
    all_gather x1, waiting for transfers between devices, body(): lax.all_gather(grids[2], 'gr', axis=2, tiled=True)  21.9 us
    all_gather x1, waiting for transfers between devices, body(): lax.all_gather(grids[1], 'gr', axis=2, tiled=True)  21.6 us
    all_gather x1, waiting for transfers between devices, body(): lax.all_gather(grids[0], 'gr', axis=2, tiled=True)  17.2 us
    all_to_all x1, blocking collectives, body(): lax.all_to_all(grids[0], 'fs', split_axis=0, concat_axis=4, tiled=True)  16.6 us
    all_to_all x1, waiting for transfers between devices, body(): lax.all_to_all(grids[1], 'fs', split_axis=0, concat_axis=4, tiled=True)  9.78 us
    all_to_all x1, waiting for transfers between devices, body(): lax.all_to_all(grids[2], 'fs', split_axis=0, concat_axis=4, tiled=True)  9.51 us
    all_to_all x1, starting transfers between devices, body(): lax.all_to_all(outgoing, ('fs', 'tp'), split_axis=0, concat_axis=0, tiled...  8.1 us
  transfers between devices with their start and end apart: 10, of which 9 were waited for; matrix products, arithmetic and copies ran while one was open for 10% of the time, Pallas kernels for 0%

commit v1 on v0

--- a/solution.py
+++ b/solution.py
@@ -52,7 +52,9 @@
     )
     grids = (
         lax.all_gather(grids[0], "gr", axis=2, tiled=True),
-        lax.all_gather(grids[1], "gr", axis=2, tiled=True),
+        jnp.concatenate(
+            lax.all_to_all(jnp.stack([grids[1]] * lax.axis_size("gr")), "gr", 0, 0), axis=2
+        ),
         lax.all_gather(grids[2], "gr", axis=2, tiled=True),
     )
 

time: 241 us -> 229 us (0.950)
  waiting for transfers between devices: 125 us -> 107 us
  starting transfers between devices: 43.7 us -> 47.8 us
    all_to_all x1, waiting for transfers between devices: 0.01 us -> 33.7 us  [body(): lax.all_to_all(outgoing, ('fs', 'tp'), split_axis=0, concat_axis=0, tiled...]
    all_gather x1, waiting for transfers between devices: 21.9 us -> 0.02 us  [body(): lax.all_gather(grids[2], 'gr', axis=2, tiled=True)]
    all_gather x1 -> x0, waiting for transfers between devices: 21.6 us -> none  [body(): lax.all_gather(grids[1], 'gr', axis=2, tiled=True)]
    all_gather x1, waiting for transfers between devices: 17.2 us -> 4.16 us  [body(): lax.all_gather(grids[0], 'gr', axis=2, tiled=True)]
    all_to_all x0 -> x1, waiting for transfers between devices: none -> 6.1 us  [body(): lax.all_to_all(jnp.stack([grids[1]] * lax.axis_size('gr')), 'gr', 0, 0)]
    all_to_all x0 -> x1, starting transfers between devices: none -> 4.42 us  [body(): lax.all_to_all(jnp.stack([grids[1]] * lax.axis_size('gr')), 'gr', 0, 0)]
  transfers between devices with their start and end apart: 10 -> 10, of which waited for: 9 -> 9; matrix products, arithmetic and copies ran while one was open for 10% -> 11% of each run, Pallas kernels for 0% -> 0%
where the time goes in v1:
time: 229 us; the launch traced here: 228 us
  waiting for transfers between devices  107 us (47%)
  starting transfers between devices  47.8 us (21%)
  local copies, waits for them, and re-layouts  26.2 us (11%)
  blocking collectives  16.6 us (7%)
  between operations  14.2 us (6%)
  other arithmetic  9.55 us (4%)
  matrix products  6.38 us (3%)
    all_to_all x1, waiting for transfers between devices, body(): lax.all_to_all(outgoing, ('fs', 'tp'), split_axis=0, concat_axis=0, tiled...  33.7 us
    all_to_all x1, waiting for transfers between devices, body(): lax.all_to_all(outcome, ('fs', 'tp'), split_axis=0, concat_axis=0, tiled=...  30 us
    all_to_all x1, blocking collectives, body(): lax.all_to_all(grids[0], 'fs', split_axis=0, concat_axis=4, tiled=True)  16.6 us
    all_to_all x1, waiting for transfers between devices, body(): lax.all_to_all(grids[1], 'fs', split_axis=0, concat_axis=4, tiled=True)  9.78 us
    all_to_all x1, waiting for transfers between devices, body(): lax.all_to_all(grids[2], 'fs', split_axis=0, concat_axis=4, tiled=True)  9.51 us
    all_to_all x1, starting transfers between devices, body(): lax.all_to_all(outgoing, ('fs', 'tp'), split_axis=0, concat_axis=0, tiled...  8.1 us
    all_to_all x1, starting transfers between devices, body(): lax.all_to_all(grids[2], 'fs', split_axis=0, concat_axis=4, tiled=True)  6.98 us
    all_to_all x1, starting transfers between devices, body(): lax.all_to_all(outcome, ('fs', 'tp'), split_axis=0, concat_axis=0, tiled=...  6.28 us
  transfers between devices with their start and end apart: 10, of which 9 were waited for; matrix products, arithmetic and copies ran while one was open for 11% of the time, Pallas kernels for 0%

profile of v1, /device:TPU:13, one launch (start us, length us, event | category | flops | bytes accessed | tf_op | source)
XLA Modules:
  0.0 227.9 jit_solution(7191702039318484158)
XLA Ops:
  7.2 2.6 %multiply_convert_fusion = (bf16[16,512,32]{1,2,0:T(8,128)(2,1)}, bf16[16,512,32]{1,2,0:T(8,128)(2,1)S(1)}) fusion(f32[16,512,32]{1,2,0:T(8,128)} %param.11, f32[512]{0:T(512)} %param.9, f32[16,512,32]{1,2,0:T(8,128)} %param.10), kind=kLoop, calls=%fused_computation.11 | loop fusion | flops 1048576 | bytes 3147776 | tf_op jit(solution)/shard_map/convert_element_type | solution.py:19
  9.8 16.6 %all_to_all.102 = bf16[4,4,1,32,512]{4,3,1,2,0:T(8,128)(2,1)S(1)} all-to-all(bf16[4,4,1,32,512]{4,3,1,2,0:T(8,128)(2,1)S(1)} %bitcast.86), channel_id=1, replica_groups=mesh['gr'=2,'fs'=4,'tp'=4] {'fs'}, dimensions={0} | all-to-all | bytes 1048576 | tf_op jit(solution)/shard_map/all_to_all | solution.py:32
  26.4 5.3 %all-to-all-start.2 = ((bf16[4,4,1,32,512]{4,3,1,2,0:T(8,128)(2,1)}), bf16[4,4,1,32,512]{4,3,1,2,0:T(8,128)(2,1)S(1)}, u32[]{:S(2)}, u32[]{:S(2)}) async-start(bf16[4,4,1,32,512]{4,3,1,2,0:T(8,128)(2,1)} %bitcast.11), calls=%async_computation.2 | async-start | bytes 1048576 | tf_op jit(solution)/shard_map/all_to_all | solution.py:39
  32.6 9.8 %all-to-all-done.2 = bf16[4,4,1,32,512]{4,3,1,2,0:T(8,128)(2,1)S(1)} async-done(((bf16[4,4,1,32,512]{4,3,1,2,0:T(8,128)(2,1)}), bf16[4,4,1,32,512]{4,3,1,2,0:T(8,128)(2,1)S(1)}, u32[]{:S(2)}, u32[]{:S(2)}) %all-to-all-start.2) | async-done | bytes 524320 | tf_op jit(solution)/shard_map/all_to_all | solution.py:39
  42.4 7.0 %all-to-all-start.5 = ((bf16[4,4,1,64,256]{4,3,1,2,0:T(8,128)(2,1)}), bf16[4,4,1,64,256]{4,3,1,2,0:T(8,128)(2,1)S(1)}, u32[]{:S(2)}, u32[]{:S(2)}) async-start(bf16[4,4,1,64,256]{4,3,1,2,0:T(8,128)(2,1)} %bitcast.19), calls=%async_computation.5 | async-start | bytes 1048576 | tf_op jit(solution)/shard_map/all_to_all | solution.py:46
  50.5 9.5 %all-to-all-done.5 = bf16[4,4,1,64,256]{4,3,1,2,0:T(8,128)(2,1)S(1)} async-done(((bf16[4,4,1,64,256]{4,3,1,2,0:T(8,128)(2,1)}), bf16[4,4,1,64,256]{4,3,1,2,0:T(8,128)(2,1)S(1)}, u32[]{:S(2)}, u32[]{:S(2)}) %all-to-all-start.5) | async-done | bytes 524320 | tf_op jit(solution)/shard_map/all_to_all | solution.py:46
  60.0 5.4 %all-to-all-start.1 = ((bf16[1,4,1,32,2048]{4,3,2,0,1:T(8,128)(2,1)}), bf16[1,4,1,32,2048]{4,3,2,0,1:T(8,128)(2,1)S(1)}, u32[]{:S(2)}, u32[]{:S(2)}) async-start(bf16[1,4,1,32,2048]{4,3,2,0,1:T(8,128)(2,1)} %bitcast.4), calls=%async_computation.1 | async-start | bytes 1048576 | tf_op jit(solution)/shard_map/all_to_all | solution.py:31
  67.0 5.3 %all-to-all-done.1 = bf16[1,4,1,32,2048]{4,3,2,0,1:T(8,128)(2,1)S(1)} async-done(((bf16[1,4,1,32,2048]{4,3,2,0,1:T(8,128)(2,1)}), bf16[1,4,1,32,2048]{4,3,2,0,1:T(8,128)(2,1)S(1)}, u32[]{:S(2)}, u32[]{:S(2)}) %all-to-all-start.1) | async-done | bytes 524320 | tf_op jit(solution)/shard_map/all_to_all | solution.py:31
  72.4 5.3 %all-to-all-start.3 = ((bf16[1,4,1,32,2048]{4,3,2,0,1:T(8,128)(2,1)}), bf16[1,4,1,32,2048]{4,3,2,0,1:T(8,128)(2,1)S(1)}, u32[]{:S(2)}, u32[]{:S(2)}) async-start(bf16[1,4,1,32,2048]{4,3,2,0,1:T(8,128)(2,1)} %bitcast.85), calls=%async_computation.3 | async-start | bytes 1048576 | tf_op jit(solution)/shard_map/all_to_all | solution.py:38
  78.7 6.0 %all-to-all-done.3 = bf16[1,4,1,32,2048]{4,3,2,0,1:T(8,128)(2,1)S(1)} async-done(((bf16[1,4,1,32,2048]{4,3,2,0,1:T(8,128)(2,1)}), bf16[1,4,1,32,2048]{4,3,2,0,1:T(8,128)(2,1)S(1)}, u32[]{:S(2)}, u32[]{:S(2)}) %all-to-all-start.3) | async-done | bytes 524320 | tf_op jit(solution)/shard_map/all_to_all | solution.py:38
  84.6 5.9 %all-to-all-start.6 = ((bf16[1,4,1,64,1024]{4,3,2,0,1:T(8,128)(2,1)}), bf16[1,4,1,64,1024]{4,3,2,0,1:T(8,128)(2,1)}, u32[]{:S(2)}, u32[]{:S(2)}) async-start(bf16[1,4,1,64,1024]{4,3,2,0,1:T(8,128)(2,1)} %bitcast.22), calls=%async_computation.6 | async-start | bytes 1048576 | tf_op jit(solution)/shard_map/all_to_all | solution.py:45
  92.4 2.6 %scatter_custom_fusion = bf16[385,2048]{1,0:T(8,128)(2,1)S(1)} fusion(s32[256]{0:T(256)S(1)} %bitcast.90, bf16[256,2048]{1,0:T(8,128)(2,1)S(1)} %reshape.143, bf16[]{:T(256)} %constant.11.clone.1), kind=kCustom, calls=%fused_computation.13 | custom fusion | bytes 1576962 | tf_op jit(solution)/shard_map/scatter | solution.py:90
  97.6 8.1 %all-to-all-start.7 = ((bf16[16,24,2048]{2,1,0:T(8,128)(2,1)}), bf16[16,24,2048]{2,1,0:T(8,128)(2,1)S(1)}, u32[]{:S(2)}, u32[]{:S(2)}) async-start(bf16[16,24,2048]{2,1,0:T(8,128)(2,1)} %bitcast.29), calls=%async_computation.7 | async-start | bytes 3145728 | tf_op jit(solution)/shard_map/all_to_all | solution.py:93
  108.3 33.7 %all-to-all-done.7 = bf16[16,24,2048]{2,1,0:T(8,128)(2,1)S(1)} async-done(((bf16[16,24,2048]{2,1,0:T(8,128)(2,1)}), bf16[16,24,2048]{2,1,0:T(8,128)(2,1)S(1)}, u32[]{:S(2)}, u32[]{:S(2)}) %all-to-all-start.7) | async-done | bytes 1572896 | tf_op jit(solution)/shard_map/all_to_all | solution.py:93
  141.9 4.4 %all-to-all-start.4 = ((bf16[2,1,1,1,128,2048]{5,4,3,2,1,0:T(8,128)(2,1)}), bf16[2,1,1,1,128,2048]{5,4,3,2,1,0:T(8,128)(2,1)}, u32[]{:S(2)}, u32[]{:S(2)}) async-start(bf16[2,1,1,1,128,2048]{5,4,3,2,1,0:T(8,128)(2,1)} %pad_maximum_fusion), calls=%async_computation.4 | async-start | bytes 2097152 | tf_op jit(solution)/shard_map/all_to_all | solution.py:56
  146.4 2.6 %reshape.122 = bf16[2,4,64,4,256]{4,3,2,1,0:T(4,128)(2,1)} reshape(bf16[1,1,2,256,1024]{4,3,1,0,2:T(8,128)(2,1)} %all-gather.5.cloned.1.call-done) | data formatting | bytes 2097152 | tf_op jit(solution)/shard_map/reshape | solution.py:70
  152.6 4.2 %all-gather.3.cloned.1.call-done = bf16[1,1,2,128,2048]{4,3,1,0,2:T(8,128)(2,1)} async-done(((bf16[1,1,1,128,2048]{4,3,1,0,2:T(8,128)(2,1)}), bf16[1,1,2,128,2048]{4,3,1,0,2:T(8,128)(2,1)}) %all-gather.3.cloned.1.call-update) | async-done | bytes 1048592 | tf_op jit(solution)/shard_map/all_gather | solution.py:54
  158.6 6.1 %all-to-all-done.4 = bf16[2,1,1,1,128,2048]{5,4,3,2,1,0:T(8,128)(2,1)} async-done(((bf16[2,1,1,1,128,2048]{5,4,3,2,1,0:T(8,128)(2,1)}), bf16[2,1,1,1,128,2048]{5,4,3,2,1,0:T(8,128)(2,1)}, u32[]{:S(2)}, u32[]{:S(2)}) %all-to-all-start.4) | async-done | bytes 1048608 | tf_op jit(solution)/shard_map/all_to_all | solution.py:56
  164.7 4.5 %convolution_convert_fusion = bf16[384,2048]{1,0:T(8,128)(2,1)} fusion(bf16[256,2048]{1,0:T(8,128)(2,1)} %squeeze_reshape.3, bf16[384,2048]{1,0:T(8,128)(2,1)S(1)} %bitcast.75, bf16[256,2048]{1,0:T(8,128)(2,1)} %bitcast.16, f32[384,256]{1,0:T(8,128)S(1)} %fusion.15), kind=kOutput, calls=%fused_computation.2 | convolution fusion | flops 806682624 | bytes 5636096 | tf_op jit(solution)/shard_map/dot_general | solution.py:98
  169.3 6.3 %all-to-all-start.8 = ((bf16[16,24,2048]{2,1,0:T(8,128)(2,1)}), bf16[16,24,2048]{2,1,0:T(8,128)(2,1)S(1)}, u32[]{:S(2)}, u32[]{:S(2)}) async-start(bf16[16,24,2048]{2,1,0:T(8,128)(2,1)} %bitcast.87), calls=%async_computation.8 | async-start | bytes 3145728 | tf_op jit(solution)/shard_map/all_to_all | solution.py:100
  175.7 2.3 copy.41
  178.0 2.3 copy.38
  181.8 30.0 %all-to-all-done.8 = bf16[16,24,2048]{2,1,0:T(8,128)(2,1)S(1)} async-done(((bf16[16,24,2048]{2,1,0:T(8,128)(2,1)}), bf16[16,24,2048]{2,1,0:T(8,128)(2,1)S(1)}, u32[]{:S(2)}, u32[]{:S(2)}) %all-to-all-start.8) | async-done | bytes 1572896 | tf_op jit(solution)/shard_map/all_to_all | solution.py:100
  217.2 3.9 %multiply_reduce_fusion = bf16[128,2048]{1,0:T(8,128)(2,1)} fusion(f32[128,2,2048]{2,1,0:T(2,128)S(1)} %reshape.130, f32[128,2]{1,0:T(8,128)S(1)} %copy.51), kind=kLoop, calls=%fused_computation.3 | loop fusion | flops 786432 | bytes 2622464 | tf_op jit(solution)/shard_map/reduce_sum | solution.py:105
  (54 shorter events, 24.1 us)
Async XLA Ops:
  9.8 22.0 %copy-start.3 = (f32[16,64,256]{2,1,0:T(8,128)S(1)}, f32[16,64,256]{2,1,0:T(8,128)}, u32[]{:S(2)}) copy-start(f32[16,64,256]{2,1,0:T(8,128)} %param.12) | copy-start | bytes 3145732
  26.4 22.9 %copy-start.6 = (s32[128]{0:T(128)S(1)}, s32[128]{0:T(128)}, u32[]{:S(2)}) copy-start(s32[128]{0:T(128)} %param.13) | copy-start | bytes 1540
  26.4 22.9 %copy-start.5 = (s32[128,2]{0,1:T(2,128)S(1)}, s32[128,2]{0,1:T(2,128)}, u32[]{:S(2)}) copy-start(s32[128,2]{0,1:T(2,128)} %param.14) | copy-start | bytes 3076
  26.4 15.9 %all-to-all-start.2 = ((bf16[4,4,1,32,512]{4,3,1,2,0:T(8,128)(2,1)}), bf16[4,4,1,32,512]{4,3,1,2,0:T(8,128)(2,1)S(1)}, u32[]{:S(2)}, u32[]{:S(2)}) async-start(bf16[4,4,1,32,512]{4,3,1,2,0:T(8,128)(2,1)} %bitcast.11), calls=%async_computation.2 | async-start | bytes 1048576 | tf_op jit(solution)/shard_map/all_to_all | solution.py:39
  42.4 23.6 %copy-start.1 = (bf16[128,2048]{1,0:T(8,128)(2,1)S(1)}, bf16[128,2048]{1,0:T(8,128)(2,1)}, u32[]{:S(2)}) copy-start(bf16[128,2048]{1,0:T(8,128)(2,1)} %param.8) | copy-start | bytes 1572868
  42.4 17.6 %all-to-all-start.5 = ((bf16[4,4,1,64,256]{4,3,1,2,0:T(8,128)(2,1)}), bf16[4,4,1,64,256]{4,3,1,2,0:T(8,128)(2,1)S(1)}, u32[]{:S(2)}, u32[]{:S(2)}) async-start(bf16[4,4,1,64,256]{4,3,1,2,0:T(8,128)(2,1)} %bitcast.19), calls=%async_computation.5 | async-start | bytes 1048576 | tf_op jit(solution)/shard_map/all_to_all | solution.py:46
  60.0 12.3 %all-to-all-start.1 = ((bf16[1,4,1,32,2048]{4,3,2,0,1:T(8,128)(2,1)}), bf16[1,4,1,32,2048]{4,3,2,0,1:T(8,128)(2,1)S(1)}, u32[]{:S(2)}, u32[]{:S(2)}) async-start(bf16[1,4,1,32,2048]{4,3,2,0,1:T(8,128)(2,1)} %bitcast.4), calls=%async_computation.1 | async-start | bytes 1048576 | tf_op jit(solution)/shard_map/all_to_all | solution.py:31
  72.4 12.3 %copy-start.2 = (bf16[1,4,1,32,2048]{4,3,2,0,1:T(8,128)(2,1)}, bf16[1,4,1,32,2048]{4,3,2,0,1:T(8,128)(2,1)S(1)}, u32[]{:S(2)}) copy-start(bf16[1,4,1,32,2048]{4,3,2,0,1:T(8,128)(2,1)S(1)} %all-to-all-done.1) | copy-start | bytes 1572868
  72.4 12.3 %all-to-all-start.3 = ((bf16[1,4,1,32,2048]{4,3,2,0,1:T(8,128)(2,1)}), bf16[1,4,1,32,2048]{4,3,2,0,1:T(8,128)(2,1)S(1)}, u32[]{:S(2)}, u32[]{:S(2)}) async-start(bf16[1,4,1,32,2048]{4,3,2,0,1:T(8,128)(2,1)} %bitcast.85), calls=%async_computation.3 | async-start | bytes 1048576 | tf_op jit(solution)/shard_map/all_to_all | solution.py:38
  84.6 13.0 %all-to-all-start.6 = ((bf16[1,4,1,64,1024]{4,3,2,0,1:T(8,128)(2,1)}), bf16[1,4,1,64,1024]{4,3,2,0,1:T(8,128)(2,1)}, u32[]{:S(2)}, u32[]{:S(2)}) async-start(bf16[1,4,1,64,1024]{4,3,2,0,1:T(8,128)(2,1)} %bitcast.22), calls=%async_computation.6 | async-start | bytes 1048576 | tf_op jit(solution)/shard_map/all_to_all | solution.py:45
  97.6 44.3 %all-to-all-start.7 = ((bf16[16,24,2048]{2,1,0:T(8,128)(2,1)}), bf16[16,24,2048]{2,1,0:T(8,128)(2,1)S(1)}, u32[]{:S(2)}, u32[]{:S(2)}) async-start(bf16[16,24,2048]{2,1,0:T(8,128)(2,1)} %bitcast.29), calls=%async_computation.7 | async-start | bytes 3145728 | tf_op jit(solution)/shard_map/all_to_all | solution.py:93
  105.7 40.7 %all-gather.5.cloned.1.call-start = ((), (), s32[]{:S(2)}) async-start(), calls=%async_computation.10 | async-start | bytes 1572864 | tf_op jit(solution)/shard_map/all_gather | solution.py:58
  106.5 50.4 %all-gather.3.cloned.1.call-start = ((), (), s32[]{:S(2)}) async-start(), calls=%async_computation.9 | async-start | bytes 1572864 | tf_op jit(solution)/shard_map/all_gather | solution.py:54
  141.9 22.8 %all-to-all-start.4 = ((bf16[2,1,1,1,128,2048]{5,4,3,2,1,0:T(8,128)(2,1)}), bf16[2,1,1,1,128,2048]{5,4,3,2,1,0:T(8,128)(2,1)}, u32[]{:S(2)}, u32[]{:S(2)}) async-start(bf16[2,1,1,1,128,2048]{5,4,3,2,1,0:T(8,128)(2,1)} %pad_maximum_fusion), calls=%async_computation.4 | async-start | bytes 2097152 | tf_op jit(solution)/shard_map/all_to_all | solution.py:56
  169.3 6.3 %copy-start.4 = (f32[128,2]{0,1:T(2,128)S(1)}, f32[128,2]{0,1:T(2,128)}, u32[]{:S(2)}) copy-start(f32[128,2]{0,1:T(2,128)} %param.15) | copy-start | bytes 3076
  169.3 42.5 %all-to-all-start.8 = ((bf16[16,24,2048]{2,1,0:T(8,128)(2,1)}), bf16[16,24,2048]{2,1,0:T(8,128)(2,1)S(1)}, u32[]{:S(2)}, u32[]{:S(2)}) async-start(bf16[16,24,2048]{2,1,0:T(8,128)(2,1)} %bitcast.87), calls=%async_computation.8 | async-start | bytes 3145728 | tf_op jit(solution)/shard_map/all_to_all | solution.py:100
  211.8 1.2 copy-start
Sparse Core Ops, SparseCore 0:
  108.1 21.7 all-gather.4
  132.0 24.7 all-gather.2
